TPU v7x, 32 devices: a whole 2x2x4 slice. The times are simulated.
32 devices in a mesh: ep: 8 (over z, x), tp: 4 (over y, core).
Axes of the slice: x: 2, y: 2, z: 4, core: 2. Of those that a mesh axis runs over, the one named last changes fastest.
Arguments:
- tokens: bfloat16 [256, 4096], P('ep'), may hold values from -6 to 6
- routes: int32 [256, 4], P('ep'), may hold values from 0 to 7, all different within a row; in each aligned block of 32 rows (0 to 31, 32 to 63, ...) at most 24 rows name the same one
- mix_weights: float32 [256, 4], P('ep'), may hold values from 0.2 to 1
- pre_gain: float32 [4096], replicated, may hold values from 0.1 to 1.9
- gate_weight: bfloat16 [8, 4096, 2048], P('ep', None, 'tp'), may hold values from -0.09375 to 0.09375
- up_weight: bfloat16 [8, 4096, 2048], P('ep', None, 'tp'), may hold values from -0.09375 to 0.09375
- down_weight: bfloat16 [8, 2048, 4096], P('ep', 'tp'), may hold values from -1 to 1
- post_gain: float32 [4096], P('tp'), may hold values from 0.1 to 1.9
Outputs:
- layer_out: bfloat16 [256, 4096], P('ep', 'tp')
Inputs may be any that keep to these rules, and one draw needn't show every extreme that they name: `routes`: within a row the 4 experts differ; among the rows of one index of ep no expert is named more than 24 times.
All inputs are finite; a program needn't handle non-finite values.
Results may differ from a plain program's by a relative error of at most 0.019.
Values may be sent and summed in bfloat16 or wider, within the bound.
A program may use at most 64 MiB of HBM per device.

v0:
```python
import functools

import jax
import jax.numpy as jnp
from jax import lax
from jax.experimental import pallas as pl
from jax.experimental.pallas import tpu as pltpu
from jax.sharding import PartitionSpec as P

epsilon = 1e-06
CORES = 2
MESH = pl.DeviceIdType.MESH
VMEM_BYTES = 60 * 1024 * 1024
MAX_COPIES = 512
SUB = 1


def fused_kernel(
    S, X, NT,
    tokens, routes, mix, pre_gain, gate_hbm, up_hbm, down_hbm, post_gain, out,
    xg, wg, wu, wd, acc_g, acc_u, hid, wt, wr,
    pown, dsend, drecv, ya, yar, xb, xbr, xa, xar, yb, ybr, keep_a, keep_b,
    za, zar, zb, zbr, st,
    wsem, ssem, gsem, mixr, dsem, yarsem, xbrsem, xarsem, ybrsem, zarsem, zbrsem, stsem,
):
    R = tokens.shape[0]
    Z, Y = S // X, NT // CORES
    Dq = xg.shape[2]
    W = 2 * SUB
    H = Dq // W
    D = tokens.shape[1]
    K = routes.shape[0]
    R2 = R // SUB
    me, t = lax.axis_index("ep"), lax.axis_index("tp")
    z, x = me // X, lax.rem(me, X)
    y, c = t // CORES, lax.rem(t, CORES)
    pc = 1 - c
    f32, bf16 = jnp.float32, jnp.bfloat16

    def dev(e, q):
        return (e, q)

    def quarter(yy, cc):
        return yy * CORES + cc

    def flip(v, m):
        for b in range(m.bit_length()):
            if m >> b & 1:
                v = v + (1 << b) * (1 - 2 * lax.rem(v // (1 << b), 2))
        return v

    if Z & (Z - 1) == 0:
        zs = [z] + [flip(z, m) for m in range(1, Z)]
        zm = zs
        near = 1
    else:
        near = 0
        zs = [lax.rem(z + d, Z) for d in range(Z)]
        zm = [lax.rem(z - d + Z, Z) for d in range(Z)]
    xs = [lax.rem(x + d, X) for d in range(X)]
    ys = [lax.rem(y + d, Y) for d in range(Y)]
    xm = [lax.rem(x - d + X, X) for d in range(X)]
    ym = [lax.rem(y - d + Y, Y) for d in range(Y)]

    loads = []
    for i in range(NT):
        for k, (src, dst) in enumerate(((gate_hbm, wg), (up_hbm, wu))):
            loads.append(pltpu.make_async_copy(src.at[0, pl.ds(i * Dq, Dq)], dst.at[i], wsem.at[k, i]))
    for i in range(NT):
        loads.append(pltpu.make_async_copy(down_hbm.at[0, :, pl.ds(i * Dq, Dq)], wd.at[i], wsem.at[2, i]))
    for copy in loads:
        copy.start()

    barrier = pltpu.get_barrier_semaphore()
    for d in range(1, S):
        pl.semaphore_signal(barrier, inc=1, device_id=dev(lax.rem(me + d, S), t), device_id_type=MESH)
    for d in range(1, NT):
        pl.semaphore_signal(barrier, inc=1, device_id=dev(me, lax.rem(t + d, NT)), device_id_type=MESH)

    floats = tokens[...].astype(f32)
    inv = lax.rsqrt(jnp.mean(floats * floats, axis=1, keepdims=True) + epsilon)
    rows = pl.ds(pl.multiple_of(me * R, R), R)
    for q in range(NT):
        cols = slice(q * Dq, (q + 1) * Dq)
        xg[q, rows, :] = (floats[:, cols] * inv * pre_gain[:, cols]).astype(bf16)

    for e in range(S):
        dense = jnp.zeros((1, R), f32)
        for k in range(K):
            dense = dense + jnp.where(routes[k : k + 1, :] == e, mix[k : k + 1, :], 0.0)
        wt[e] = jnp.concatenate([dense, jnp.zeros((1, 128 - R), f32)], axis=1)
    wr[me] = wt[me]

    pl.semaphore_wait(barrier, S - 1 + NT - 1)

    sends = []

    def send(src, dst, recv_sem, device):
        copy = pltpu.make_async_remote_copy(
            src_ref=src, dst_ref=dst, send_sem=ssem.at[len(sends)], recv_sem=recv_sem,
            device_id=device, device_id_type=MESH,
        )
        copy.start()
        sends.append(copy)

    def arrived(ref, sem):
        pltpu.make_async_remote_copy(
            src_ref=ref, dst_ref=ref, send_sem=ssem.at[0], recv_sem=sem,
            device_id=dev(me, t), device_id_type=MESH,
        ).wait_recv()

    def block(q, s, i):
        return xg.at[q, pl.ds(pl.multiple_of(s * R + i * R2, R2), R2)]

    def send_block(q, s, i, device):
        send(block(q, s, i), block(q, s, i), gsem.at[q, s, i], device)

    def await_block(q, s):
        for i in range(SUB):
            arrived(block(q, s, i), gsem.at[q, s, i])

    def await_part(q, s, i):
        arrived(block(q, s, i), gsem.at[q, s, i])

    def at(d, dx):
        return zm[d] * X + xm[dx]

    for d in range(1, Z):
        for i in range(SUB):
            send_block(t, me, i, dev(zs[d] * X + x, t))
            if d == near:
                for dy in range(1, Y):
                    send_block(quarter(ys[dy], c), me, i, dev(zs[d] * X + x, t))
    for dx in range(1, X):
        for i in range(SUB):
            send_block(t, me, i, dev(z * X + xs[dx], t))
            for dy in range(1, Y):
                send_block(quarter(ys[dy], c), me, i, dev(z * X + xs[dx], t))
    for d in range(1, S):
        e = lax.rem(me + d, S)
        send(wt.at[e], wr.at[me], mixr.at[me], dev(e, t))
    for d in range(1, Z):
        s = at(d, 0)
        for i in range(SUB):
            await_part(t, s, i)
            for dx in range(1, X):
                send_block(t, s, i, dev(z * X + xs[dx], t))
            if d != near:
                for dy in range(1, Y):
                    send_block(t, s, i, dev(me, quarter(ys[dy], c)))
            send_block(t, s, i, dev(me, quarter(y, pc)))
            if d == near:
                for dy in range(1, Y):
                    q = quarter(ys[dy], c)
                    await_part(q, s, i)
                    for dx in range(1, X):
                        send_block(q, s, i, dev(z * X + xs[dx], t))
                    send_block(q, s, i, dev(me, quarter(y, pc)))
    for dx in range(1, X):
        for d in range(Z):
            s = at(d, dx)
            for i in range(SUB):
                await_part(t, s, i)
                if d not in (0, near):
                    for dy in range(1, Y):
                        send_block(t, s, i, dev(me, quarter(ys[dy], c)))
                send_block(t, s, i, dev(me, quarter(y, pc)))
                if d in (0, near):
                    for dy in range(1, Y):
                        await_part(quarter(ys[dy], c), s, i)
                        send_block(quarter(ys[dy], c), s, i, dev(me, quarter(y, pc)))

    others = [at(d, dx) for dx in range(X) for d in range(Z) if d or dx]

    def multiply(q, first):
        pltpu.make_async_copy(gate_hbm.at[0, pl.ds(0, Dq)], wg.at[q], wsem.at[0, q]).wait()
        pltpu.make_async_copy(up_hbm.at[0, pl.ds(0, Dq)], wu.at[q], wsem.at[1, q]).wait()
        for w, acc in ((wg, acc_g), (wu, acc_u)):
            part = jnp.dot(xg[q], w[q], preferred_element_type=f32)
            acc[...] = part if first else acc[...] + part

    multiply(t, True)
    for s in others:
        await_block(quarter(y, pc), s)
    multiply(quarter(y, pc), False)
    for dy in range(1, Y):
        for dx in range(X):
            for d in range(1, Z):
                if d == near:
                    continue
                s = at(d, dx)
                for i in range(SUB):
                    await_part(quarter(ym[dy], c), s, i)
                    send_block(quarter(ym[dy], c), s, i, dev(me, quarter(y, pc)))
        multiply(quarter(ym[dy], c), False)
    for dy in range(1, Y):
        for s in others:
            await_block(quarter(ym[dy], pc), s)
        multiply(quarter(ym[dy], pc), False)

    for d in range(1, S):
        s = lax.rem(me + d, S)
        arrived(wr.at[s], mixr.at[s])
    named = jnp.concatenate([wr[s] for s in range(S)] + [jnp.zeros((128 - S, 128), f32)], axis=0)
    columns = jnp.transpose(named)
    weight = jnp.concatenate([columns[:R, s : s + 1] for s in range(S)], axis=0)
    gate = acc_g[...]
    hid[...] = (gate / (1.0 + jnp.exp(-gate)) * acc_u[...] * weight).astype(bf16)

    def down(q):
        pltpu.make_async_copy(down_hbm.at[0, :, pl.ds(0, Dq)], wd.at[q], wsem.at[2, q]).wait()
        return jnp.dot(hid[...], wd[q], preferred_element_type=f32)

    y_order = [ys[dy] for dy in range(1, Y)] + [y]
    js = [zs[d] for d in range(1, Z)] + [z]
    first, second = list(range(SUB)), list(range(SUB, W))

    def own(yy, h, j, xx):
        return pown[yy, h, j, xx] + drecv[yy, h, j, xx].astype(f32)

    def await_core(yy, h):
        arrived(drecv.at[yy, h], dsem.at[yy, h])

    for dy in list(range(1, Y)) + [0]:
        yy = ys[dy]
        part = down(quarter(yy, pc)).astype(bf16)
        for h in first + second if dy else second + first:
            for s in range(S):
                dsend[yy, h, s // X, s % X] = part[s * R : (s + 1) * R, h * H : (h + 1) * H]
            send(dsend.at[yy, h], drecv.at[yy, h], dsem.at[yy, h], dev(me, quarter(y, pc)))
        part = down(quarter(yy, c))
        for h in range(W):
            for s in range(S):
                pown[yy, h, s // X, s % X] = part[s * R : (s + 1) * R, h * H : (h + 1) * H]
        if dy:
            for h in first:
                await_core(yy, h)
            for j in js:
                for h in first:
                    for xx in range(X):
                        ya[dy, h, j, xx] = own(yy, h, j, xx).astype(bf16)
                    send(ya.at[dy, h, j], yar.at[dy, h, j], yarsem.at[dy, h, j], dev(me, quarter(yy, c)))
        for h in second:
            await_core(yy, h)
        for j in js:
            for h in second:
                for dx in range(1, X):
                    xb[dx, yy, h - SUB, j] = own(yy, h, j, xs[dx]).astype(bf16)
                    send(
                        xb.at[dx, yy, h - SUB, j], xbr.at[dx, yy, h - SUB, j],
                        xbrsem.at[dx, yy, h - SUB, j], dev(z * X + xs[dx], t),
                    )
    for h in first:
        await_core(y, h)
    for j in js:
        for i in range(SUB):
            for yy in y_order:
                total = own(yy, SUB + i, j, x)
                for dx in range(1, X):
                    arrived(xbr.at[dx, yy, i, j], xbrsem.at[dx, yy, i, j])
                    total = total + xbr[dx, yy, i, j].astype(f32)
                keep_b[yy, i, j] = total
            for dy in range(1, Y):
                yb[dy, i, j] = keep_b[ys[dy], i, j].astype(bf16)
                send(yb.at[dy, i, j], ybr.at[dy, i, j], ybrsem.at[dy, i, j], dev(me, quarter(ys[dy], c)))
            for dy in range(1, Y):
                arrived(yar.at[dy, i, j], yarsem.at[dy, i, j])
            for dx in list(range(1, X)) + [0]:
                total = own(y, i, j, xs[dx])
                for dy in range(1, Y):
                    total = total + yar[dy, i, j, xs[dx]].astype(f32)
                if dx == 0:
                    keep_a[i, j] = total
                else:
                    xa[dx, i, j] = total.astype(bf16)
                    send(xa.at[dx, i, j], xar.at[dx, i, j], xarsem.at[dx, i, j], dev(z * X + xs[dx], t))
    mine = {}
    for at_d, j in enumerate(js):
        d = (at_d + 1) % Z
        for i in range(SUB):
            total = keep_a[i, j]
            for dx in range(1, X):
                arrived(xar.at[dx, i, j], xarsem.at[dx, i, j])
                total = total + xar[dx, i, j].astype(f32)
            if d:
                za[d, i] = total.astype(bf16)
                send(za.at[d, i], zar.at[d, i], zarsem.at[d, i], dev(j * X + x, t))
            else:
                mine[i] = total
            total = keep_b[y, i, j]
            for dy in range(1, Y):
                arrived(ybr.at[dy, i, j], ybrsem.at[dy, i, j])
                total = total + ybr[dy, i, j].astype(f32)
            if d:
                zb[d, i] = total.astype(bf16)
                send(zb.at[d, i], zbr.at[d, i], zbrsem.at[d, i], dev(j * X + x, t))
            else:
                mine[SUB + i] = total
    for d in range(1, Z):
        for i in range(SUB):
            arrived(zar.at[d, i], zarsem.at[d, i])
            mine[i] = mine[i] + zar[d, i].astype(f32)
            arrived(zbr.at[d, i], zbrsem.at[d, i])
            mine[SUB + i] = mine[SUB + i] + zbr[d, i].astype(f32)

    squares = jnp.zeros((R, 1), f32)
    for h in range(W):
        squares = squares + jnp.sum(mine[h] * mine[h], axis=1, keepdims=True)
    st[0] = jnp.broadcast_to(squares, (R, 128))
    for d in range(1, NT):
        send(st.at[0], st.at[d], stsem.at[d], dev(me, lax.rem(t + d, NT)))
    for d in range(1, NT):
        arrived(st.at[d], stsem.at[d])
        squares = squares + st[d][:, 0:1]
    scale = lax.rsqrt(squares / D + epsilon)
    for h in range(W):
        cols = slice(h * H, (h + 1) * H)
        out[:, cols] = (mine[h] * scale * post_gain[:, cols]).astype(bf16)
    for copy in sends:
        copy.wait_send()


def fused(S, X, NT, tokens, routes, mix_weights, pre_gain, gate_weight, up_weight, down_weight, post_gain):
    R, D = tokens.shape
    F = gate_weight.shape[2]
    Dq = D // NT
    W = 2 * SUB
    H = Dq // W
    Z, Y = S // X, NT // CORES
    f32, bf16 = jnp.float32, jnp.bfloat16
    dma, vmem = pltpu.SemaphoreType.DMA, pltpu.VMEM
    in_vmem, anywhere = pl.BlockSpec(memory_space=pltpu.VMEM), pl.BlockSpec(memory_space=pl.ANY)
    return pl.pallas_call(
        functools.partial(fused_kernel, S, X, NT),
        out_shape=jax.ShapeDtypeStruct((R, Dq), bf16),
        in_specs=[in_vmem] * 4 + [anywhere] * 3 + [in_vmem],
        out_specs=in_vmem,
        scratch_shapes=[
            vmem((NT, S * R, Dq), bf16),
            vmem((NT, Dq, F), bf16),
            vmem((NT, Dq, F), bf16),
            vmem((NT, F, Dq), bf16),
            vmem((S * R, F), f32),
            vmem((S * R, F), f32),
            vmem((S * R, F), bf16),
            vmem((S, 1, 128), f32),
            vmem((S, 1, 128), f32),
            vmem((Y, W, Z, X, R, H), f32),
            vmem((Y, W, Z, X, R, H), bf16),
            vmem((Y, W, Z, X, R, H), bf16),
            vmem((Y, SUB, Z, X, R, H), bf16),
            vmem((Y, SUB, Z, X, R, H), bf16),
            vmem((X, Y, SUB, Z, R, H), bf16),
            vmem((X, Y, SUB, Z, R, H), bf16),
            vmem((X, SUB, Z, R, H), bf16),
            vmem((X, SUB, Z, R, H), bf16),
            vmem((Y, SUB, Z, R, H), bf16),
            vmem((Y, SUB, Z, R, H), bf16),
            vmem((SUB, Z, R, H), f32),
            vmem((Y, SUB, Z, R, H), f32),
            vmem((Z, SUB, R, H), bf16),
            vmem((Z, SUB, R, H), bf16),
            vmem((Z, SUB, R, H), bf16),
            vmem((Z, SUB, R, H), bf16),
            vmem((NT, R, 128), f32),
            dma((3, NT)),
            dma((copies_of(S, X, NT),)),
            dma((NT, S, SUB)),
            dma((S,)),
            dma((Y, W)),
            dma((Y, SUB, Z)),
            dma((X, Y, SUB, Z)),
            dma((X, SUB, Z)),
            dma((Y, SUB, Z)),
            dma((Z, SUB)),
            dma((Z, SUB)),
            dma((NT,)),
        ],
        compiler_params=pltpu.CompilerParams(
            collective_id=0, has_side_effects=True, vmem_limit_bytes=VMEM_BYTES
        ),
    )(
        tokens, routes.T, mix_weights.T, pre_gain.reshape(1, D), gate_weight, up_weight, down_weight,
        post_gain.reshape(1, Dq),
    )


def routed(
    tokens, routes, mix_weights, pre_gain, gate_weight, up_weight, down_weight, post_gain
):
    tok_rows, width = tokens.shape
    top_count = routes.shape[1]
    experts = lax.axis_size("ep")
    capacity = min(tok_rows, max(2, (3 * tok_rows * top_count + 2 * experts - 1) // (2 * experts)))
    floats = tokens.astype(jnp.float32)
    normed = (
        floats * lax.rsqrt(jnp.mean(floats * floats, axis=-1, keepdims=True) + epsilon) * pre_gain
    ).astype(jnp.bfloat16)
    chosen = routes.reshape(-1)
    onehot = (chosen[:, None] == jnp.arange(experts, dtype=jnp.int32)[None, :]).astype(jnp.int32)
    before = jnp.cumsum(onehot, axis=0) - onehot
    slot_rank = jnp.sum(before * onehot, axis=1)
    target = chosen * capacity + slot_rank
    placed = target[:, None] == jnp.arange(experts * capacity, dtype=jnp.int32)[None, :]
    by_choice = placed.reshape(tok_rows, top_count, experts * capacity)
    picked = jnp.any(by_choice, axis=1).astype(jnp.bfloat16)
    outgoing = jnp.einsum("tc,td->cd", picked, normed, preferred_element_type=jnp.float32).astype(
        jnp.bfloat16
    )
    outgoing = outgoing.reshape(experts, capacity, width)
    slice_width = width // lax.axis_size("tp")
    outgoing_part = lax.dynamic_slice_in_dim(
        outgoing, lax.axis_index("tp") * slice_width, slice_width, 2
    )
    arrived = lax.all_to_all(outgoing_part, "ep", split_axis=0, concat_axis=0, tiled=True)
    arrived = lax.all_gather(arrived, "tp", axis=2, tiled=True)
    arrived_rows = arrived.reshape(experts * capacity, width)
    gate_act = jnp.dot(arrived_rows, gate_weight[0], preferred_element_type=jnp.float32)
    up_act = jnp.dot(arrived_rows, up_weight[0], preferred_element_type=jnp.float32)
    hidden = (jax.nn.silu(gate_act) * up_act).astype(jnp.bfloat16)
    partial_value = jnp.dot(hidden, down_weight[0], preferred_element_type=jnp.float32)
    summed = lax.psum_scatter(
        partial_value.astype(jnp.bfloat16), "tp", scatter_dimension=1, tiled=True
    )
    returned = lax.all_to_all(
        summed.reshape(experts, capacity, summed.shape[1]),
        "ep",
        split_axis=0,
        concat_axis=0,
        tiled=True,
    )
    results = returned.reshape(experts * capacity, summed.shape[1]).astype(jnp.float32)
    mixing = jnp.sum(mix_weights[:, :, None] * by_choice.astype(jnp.float32), axis=1)
    mixed = jnp.dot(mixing, results, precision=lax.Precision.HIGHEST)
    squares = jnp.sum(mixed * mixed, axis=1)
    total = lax.psum(squares, "tp")
    scale = lax.rsqrt(total / width + epsilon)
    return (mixed * scale[:, None] * post_gain).astype(jnp.bfloat16)


def copies_of(S, X, NT):
    Z, Y = S // X, NT // CORES
    gather = SUB * ((Z - 1 + X - 1) * Y + 3 * NT * S) + S - 1
    back = Y * 2 * SUB + SUB * Z * (2 * (Y - 1) + (X - 1) * (Y + 1) + 2) + NT
    return gather + back


def solution(mesh):
    in_specs = (
        P("ep", None),
        P("ep", None),
        P("ep", None),
        P(),
        P("ep", None, "tp"),
        P("ep", None, "tp"),
        P("ep", "tp", None),
        P("tp"),
    )
    out_specs = P("ep", "tp")
    S, NT = mesh.shape["ep"], mesh.shape["tp"]
    X = 2
    on_device = routed
    if S % X == 0 and NT % CORES == 0 and copies_of(S, X, NT) <= MAX_COPIES:
        on_device = functools.partial(fused, S, X, NT)
    return jax.shard_map(
        on_device, mesh=mesh, in_specs=in_specs, out_specs=out_specs, check_vma=False
    )
```

profile of v0, /device:TPU:0, one launch (start us, length us, event | category | flops | bytes accessed | tf_op | source)
XLA Modules:
  0.0 47.8 jit_solution(13463269120194612800)
XLA Ops:
  0.0 46.3 %shard_map.82 = bf16[32,1024]{1,0:T(8,128)(2,1)} custom-call(bf16[32,4096]{1,0:T(8,128)(2,1)} %tokens.1, s32[4,32]{1,0:T(4,128)} %bitcast.6, f32[4,32]{1,0:T(4,128)} %bitcast.7, f32[1,4096]{1,0:T(1,128)} %bitcast.4, bf16[1,4096,512]{2,1,0:T(8,128)(2,1)} %gate_hbm.1, bf16[1,4096,512]{2,1,0:T(8,128)(2,1)} %up_hbm.1, bf16[1,512,4096]{2,1,0:T(8,128)(2,1)} %down_hbm.1, ...), custom_call_target="tpu_custom_call" | custom-call | tf_op jit(solution)/shard_map/pallas_call | solution.py:333
  46.3 1.5 %copy.10 = bf16[32,1024]{1,0:T(8,128)(2,1)} copy(bf16[32,1024]{1,0:T(8,128)(2,1)} %shard_map.82) | data formatting | bytes 131072
where the time goes:
time: 47.9 us; the launch traced here: 47.8 us
  Pallas kernels  46.3 us (97%)
  local copies, waits for them, and re-layouts  1.47 us (3%)
    pallas_call x1, Pallas kernels, fused(): pl.pallas_call(functools.partial(fused_kernel, S, X, NT), out_shape=jax.S...  46.3 us
    unnamed x1, local copies, waits for them, and re-layouts  1.47 us

commit v1 on v0

v1 whole, which is shorter than its diff:
```python
import functools

import jax
import jax.numpy as jnp
from jax import lax
from jax.experimental import pallas as pl
from jax.experimental.pallas import tpu as pltpu
from jax.sharding import PartitionSpec as P

epsilon = 1e-06
CORES = 2
MESH = pl.DeviceIdType.MESH
VMEM_BYTES = 60 * 1024 * 1024
SUB = 1
OUT = [('z', 1), ('x', 0), ('z', 2), ('z', 3), ('xb', 0), ('zb', 1)]
XB = []
EVENTS = [('x', 0, 0), ('z', 1, 0), ('z', 2, 0), ('z', 3, 0), ('x', 1, 0), ('x', 2, 0), ('x', 3, 0), ('v', 1, 0), ('v', 2, 0), ('w', 0, 0), ('v', 3, 0), ('w', 1, 0), ('w', 2, 0), ('w', 3, 0)]


def fused_kernel(
    S, X, NT,
    tokens_hbm, routes_hbm, mix_hbm, pre_hbm, gate_hbm, up_hbm, down_hbm, post_hbm, out,
    tok, rt, mx, pre, post, xg, wg, wu, wd, wp, acc_g, acc_u, hid, hidp, wt, wr, weight,
    part, ya, yar, xb, xbr, xa, xar, yb, ybr, keep_a, keep_b, za, zar, zb, zbr, st,
    insem, wsem, ssem, gsem, psem, mixsem, hidsem, yarsem, xbrsem, xarsem, ybrsem, zsem, stsem,
):
    R, Dq = tok.shape[1], tok.shape[2]
    D = Dq * NT
    Z = S // X
    H = Dq // 2
    K = rt.shape[0]
    R2 = R // SUB
    me, t = lax.axis_index("ep"), lax.axis_index("tp")
    z, x = me // X, lax.rem(me, X)
    y, c = t // CORES, lax.rem(t, CORES)
    f32, bf16 = jnp.float32, jnp.bfloat16

    def flip(v, m):
        for b in range(m.bit_length()):
            if m >> b & 1:
                v = v + (1 << b) * (1 - 2 * lax.rem(v // (1 << b), 2))
        return v

    zs, xs, ys = [flip(z, d) for d in range(Z)], [x, 1 - x], [y, 1 - y]
    cs = [c, 1 - c]
    quarters = [ys[0] * CORES + cs[0], ys[0] * CORES + cs[1], ys[1] * CORES + cs[0], ys[1] * CORES + cs[1]]

    def peer(d, dx):
        return (zs[d] * X + xs[dx], t)

    across, partner = (me, quarters[2]), (me, quarters[1])
    beside = peer(0, 1)

    barrier = pltpu.get_barrier_semaphore()
    everyone = [peer(d, dx) for d in range(Z) for dx in range(X) if d or dx] + [(me, q) for q in quarters[1:]]
    for device in everyone:
        pl.semaphore_signal(barrier, inc=1, device_id=device, device_id_type=MESH)

    def span(q):
        return pl.ds(pl.multiple_of(q * Dq, Dq), Dq)

    first = [pltpu.make_async_copy(tokens_hbm.at[:, span(q)], tok.at[k], insem.at[0]) for k, q in enumerate(quarters)]
    first += [pltpu.make_async_copy(pre_hbm.at[:, span(q)], pre.at[k], insem.at[1]) for k, q in enumerate(quarters)]
    second = [
        pltpu.make_async_copy(routes_hbm, rt, insem.at[2]),
        pltpu.make_async_copy(mix_hbm, mx, insem.at[3]),
        pltpu.make_async_copy(post_hbm, post, insem.at[4]),
    ]
    for copy in first + second:
        copy.start()
    pltpu.make_async_copy(tok, tok, insem.at[0]).wait()
    pltpu.make_async_copy(pre, pre, insem.at[1]).wait()
    for copy in second:
        copy.wait()
    for k, q in enumerate(quarters):
        pltpu.make_async_copy(gate_hbm.at[0, span(q)], wg.at[k], wsem.at[k]).start()
        pltpu.make_async_copy(up_hbm.at[0, span(q)], wu.at[k], wsem.at[k]).start()
    for k, q in enumerate((quarters[0], quarters[2])):
        pltpu.make_async_copy(down_hbm.at[0, :, span(q)], wd.at[k], wsem.at[NT + k]).start()

    squares = jnp.zeros((R, 1), f32)
    for k in range(NT):
        floats = tok[k].astype(f32)
        squares = squares + jnp.sum(floats * floats, axis=1, keepdims=True)
    inv = lax.rsqrt(squares / D + epsilon)
    for k in range(NT):
        xg[k, 0:R, :] = (tok[k].astype(f32) * inv * pre[k]).astype(bf16)

    chosen, mixing = rt[...], mx[...]
    for d in range(Z):
        for dx in range(X):
            e = zs[d] * X + xs[dx]
            dense = jnp.zeros((1, R), f32)
            for k in range(K):
                dense = dense + jnp.where(chosen[k : k + 1, :] == e, mixing[k : k + 1, :], 0.0)
            wt[d * X + dx] = jnp.concatenate([dense, jnp.zeros((1, 128 - R), f32)], axis=1)
    wr[0] = wt[0]

    sent = [0, 0, 0]

    def bytes_of(ref):
        n = 1
        for size in ref.shape:
            n *= size
        return n * jnp.dtype(ref.dtype).itemsize

    def send(group, src, dst, recv_sem, device):
        pltpu.make_async_remote_copy(
            src_ref=src, dst_ref=dst, send_sem=ssem.at[group], recv_sem=recv_sem,
            device_id=device, device_id_type=MESH,
        ).start()
        sent[group] += bytes_of(src)

    def arrived(ref, sem):
        pltpu.make_async_copy(ref, ref, sem).wait()

    def block(k, b, i):
        return xg.at[k, b * R + i * R2 : b * R + (i + 1) * R2]

    def slot(half, b, i):
        return gsem.at[(half * (S - 1) + b - 1) * SUB + i]

    pl.semaphore_wait(barrier, len(everyone))

    for i in range(SUB):
        for kind, d in OUT:
            if kind == "z":
                send(0, block(0, 0, i), block(0, d * X, i), slot(0, d * X, i), peer(d, 0))
            elif kind == "zb":
                send(0, block(2, 0, i), block(2, d * X, i), slot(1, d * X, i), peer(d, 0))
            elif kind == "x":
                send(0, block(0, 0, i), block(0, 1, i), slot(0, 1, i), beside)
            elif kind == "xb":
                send(0, block(2, 0, i), block(2, 1, i), slot(1, 1, i), beside)
    for k, q in enumerate((quarters[1], quarters[3])):
        send(1, down_hbm.at[0, :, span(q)], wp.at[k], wsem.at[NT + 2 + k], partner)
    for b in range(1, S):
        send(2, wt.at[b], wr.at[b], mixsem.at[0], peer(b // X, b % X))

    by_z = [d for kind, d in OUT if kind == "zb"]
    by_x = [0] * any(kind == "xb" for kind, d in OUT) + XB

    def handle(kind, d, i):
        dx = 1 if kind[0] in "xw" else 0
        half = 0 if kind in "zx" else 1
        b = d * X + dx
        arrived(block(2 * half, b, i), slot(half, b, i))
        if dx == 0 and (half == 0 or d in by_x):
            send(0, block(2 * half, b, i), block(2 * half, b + 1, i), slot(half, b + 1, i), beside)
        if half == 0 and d not in (by_x if dx else by_z):
            send(0, block(0, b, i), block(2, b, i), slot(1, b, i), across)
        send(0, block(2 * half, b, i), block(2 * half + 1, b, i), psem.at[half], partner)

    def run(events):
        for kind, d, i in events:
            handle(kind, d, i)

    def multiply(k, start):
        both = pltpu.make_async_copy(wg.at[0], wg.at[0], wsem.at[k])
        both.wait()
        both.wait()
        for w, acc in ((wg, acc_g), (wu, acc_u)):
            product = jnp.dot(xg[k], w[k], preferred_element_type=f32)
            acc[...] = product if start else acc[...] + product

    late = [e for e in EVENTS if not (e[0] in "zx")]
    cut = max(n for n, e in enumerate(EVENTS) if e[0] in "zx") + 1
    run(EVENTS[:cut])
    multiply(0, True)
    arrived(xg.at[1, R : S * R], psem.at[0])
    multiply(1, False)
    arrived(wr.at[1:S], mixsem.at[0])
    named = jnp.concatenate([wr[b] for b in range(S)] + [jnp.zeros((128 - S, 128), f32)], axis=0)
    columns = jnp.transpose(named)
    for b in range(S):
        weight[b * R : (b + 1) * R] = jnp.broadcast_to(columns[:R, b : b + 1], (R, 128))
    run(EVENTS[cut:])
    multiply(2, False)
    arrived(xg.at[3, R : S * R], psem.at[1])
    multiply(3, False)

    F = hid.shape[1]
    half_rows = S * R // 2
    for i in range(2):
        rows = slice(i * half_rows, (i + 1) * half_rows)
        for at in range(0, F, 128):
            cols = slice(at, at + 128)
            gate = acc_g[rows, cols]
            hid[rows, cols] = (gate / (1.0 + jnp.exp(-gate)) * acc_u[rows, cols] * weight[rows]).astype(bf16)
        send(1, hid.at[rows], hidp.at[rows], hidsem.at[i], partner)
    for k in (1, 0):
        arrived(wd.at[k], wsem.at[NT + k])
        part[k] = jnp.dot(hid[...], wd[k], preferred_element_type=f32)
    for k in (1, 0):
        arrived(wp.at[k], wsem.at[NT + 2 + k])
    for i in range(2):
        rows = slice(i * half_rows, (i + 1) * half_rows)
        arrived(hidp.at[rows], hidsem.at[i])
    order = [d for d in range(1, Z)] + [0]
    for k in (1, 0):
        part[k] = part[k] + jnp.dot(hidp[...], wp[k], preferred_element_type=f32)
        for d in order:
            for dx in range(X):
                b = d * X + dx
                rows = slice(b * R, (b + 1) * R)
                if k:
                    ya[b] = part[k, rows, :H].astype(bf16)
                    send(1, ya.at[b], yar.at[b], yarsem.at[d], across)
                if dx:
                    xb[k, d] = part[k, rows, H:].astype(bf16)
                    send(1, xb.at[k, d], xbr.at[k, d], xbrsem.at[d], beside)

    for d in order:
        arrived(yar.at[d * X : (d + 1) * X], yarsem.at[d])
        for dx in (1, 0):
            b = d * X + dx
            total = part[0, b * R : (b + 1) * R, :H] + yar[b].astype(f32)
            if dx:
                xa[d] = total.astype(bf16)
                send(1, xa.at[d], xar.at[d], xarsem.at[d], beside)
            else:
                keep_a[d] = total
        arrived(xbr.at[:, d], xbrsem.at[d])
        for k in (1, 0):
            rows = slice(d * X * R, (d * X + 1) * R)
            total = part[k, rows, H:] + xbr[k, d].astype(f32)
            if k:
                yb[d] = total.astype(bf16)
                send(1, yb.at[d], ybr.at[d], ybrsem.at[d], across)
            else:
                keep_b[d] = total
    for d in order:
        arrived(xar.at[d], xarsem.at[d])
        total = keep_a[d] + xar[d].astype(f32)
        if d:
            za[d] = total.astype(bf16)
            send(1, za.at[d], zar.at[d], zsem.at[2 * d - 2], peer(d, 0))
        else:
            mine_a = total
        arrived(ybr.at[d], ybrsem.at[d])
        total = keep_b[d] + ybr[d].astype(f32)
        if d:
            zb[d] = total.astype(bf16)
            send(1, zb.at[d], zbr.at[d], zsem.at[2 * d - 1], peer(d, 0))
        else:
            mine_b = total
    for d in range(1, Z):
        arrived(zar.at[d], zsem.at[2 * d - 2])
        mine_a = mine_a + zar[d].astype(f32)
        arrived(zbr.at[d], zsem.at[2 * d - 1])
        mine_b = mine_b + zbr[d].astype(f32)

    squares = jnp.sum(mine_a * mine_a, axis=1, keepdims=True) + jnp.sum(mine_b * mine_b, axis=1, keepdims=True)
    st[0] = jnp.broadcast_to(squares, (R, 128))
    for k in range(1, NT):
        send(1, st.at[0], st.at[k], stsem.at[0], (me, quarters[k]))
    arrived(st.at[1:NT], stsem.at[0])
    for k in range(1, NT):
        squares = squares + st[k][:, 0:1]
    scale = lax.rsqrt(squares / D + epsilon)
    out[:, :H] = (mine_a * scale * post[:, :H]).astype(bf16)
    out[:, H:] = (mine_b * scale * post[:, H:]).astype(bf16)
    for group in (0, 1):
        span_of = gate_hbm.at[0, 0 : sent[group] // (2 * F)]
        arrived(span_of, ssem.at[group])
    arrived(wt.at[1:S], ssem.at[2])


def fused(S, X, NT, tokens, routes, mix_weights, pre_gain, gate_weight, up_weight, down_weight, post_gain):
    R, D = tokens.shape
    K = routes.shape[1]
    F = gate_weight.shape[2]
    Dq = D // NT
    H = Dq // 2
    Z = S // X
    f32, bf16 = jnp.float32, jnp.bfloat16
    dma, vmem = pltpu.SemaphoreType.DMA, pltpu.VMEM
    in_hbm = pl.BlockSpec(memory_space=pltpu.HBM)
    return pl.pallas_call(
        functools.partial(fused_kernel, S, X, NT),
        out_shape=jax.ShapeDtypeStruct((R, Dq), bf16),
        in_specs=[in_hbm] * 8,
        out_specs=pl.BlockSpec(memory_space=pltpu.VMEM),
        scratch_shapes=[
            vmem((NT, R, Dq), bf16),
            vmem((K, R), jnp.int32),
            vmem((K, R), f32),
            vmem((NT, 1, Dq), f32),
            vmem((1, Dq), f32),
            vmem((NT, S * R, Dq), bf16),
            vmem((NT, Dq, F), bf16),
            vmem((NT, Dq, F), bf16),
            vmem((2, F, Dq), bf16),
            vmem((2, F, Dq), bf16),
            vmem((S * R, F), f32),
            vmem((S * R, F), f32),
            vmem((S * R, F), bf16),
            vmem((S * R, F), bf16),
            vmem((S, 1, 128), f32),
            vmem((S, 1, 128), f32),
            vmem((S * R, 128), f32),
            vmem((2, S * R, Dq), f32),
            vmem((S, R, H), bf16),
            vmem((S, R, H), bf16),
            vmem((2, Z, R, H), bf16),
            vmem((2, Z, R, H), bf16),
            vmem((Z, R, H), bf16),
            vmem((Z, R, H), bf16),
            vmem((Z, R, H), bf16),
            vmem((Z, R, H), bf16),
            vmem((Z, R, H), f32),
            vmem((Z, R, H), f32),
            vmem((Z, R, H), bf16),
            vmem((Z, R, H), bf16),
            vmem((Z, R, H), bf16),
            vmem((Z, R, H), bf16),
            vmem((NT, R, 128), f32),
            dma((5,)),
            dma((NT + 4,)),
            dma((3,)),
            dma((2 * (S - 1) * SUB,)),
            dma((2,)),
            dma((1,)),
            dma((2,)),
            dma((Z,)),
            dma((Z,)),
            dma((Z,)),
            dma((Z,)),
            dma((2 * (Z - 1),)),
            dma((1,)),
        ],
        compiler_params=pltpu.CompilerParams(
            collective_id=0, has_side_effects=True, vmem_limit_bytes=VMEM_BYTES
        ),
    )(
        tokens, routes.T, mix_weights.T, pre_gain.reshape(1, D), gate_weight, up_weight, down_weight,
        post_gain.reshape(1, Dq),
    )


def routed(
    tokens, routes, mix_weights, pre_gain, gate_weight, up_weight, down_weight, post_gain
):
    tok_rows, width = tokens.shape
    top_count = routes.shape[1]
    experts = lax.axis_size("ep")
    capacity = min(tok_rows, max(2, (3 * tok_rows * top_count + 2 * experts - 1) // (2 * experts)))
    floats = tokens.astype(jnp.float32)
    normed = (
        floats * lax.rsqrt(jnp.mean(floats * floats, axis=-1, keepdims=True) + epsilon) * pre_gain
    ).astype(jnp.bfloat16)
    chosen = routes.reshape(-1)
    onehot = (chosen[:, None] == jnp.arange(experts, dtype=jnp.int32)[None, :]).astype(jnp.int32)
    before = jnp.cumsum(onehot, axis=0) - onehot
    slot_rank = jnp.sum(before * onehot, axis=1)
    target = chosen * capacity + slot_rank
    placed = target[:, None] == jnp.arange(experts * capacity, dtype=jnp.int32)[None, :]
    by_choice = placed.reshape(tok_rows, top_count, experts * capacity)
    picked = jnp.any(by_choice, axis=1).astype(jnp.bfloat16)
    outgoing = jnp.einsum("tc,td->cd", picked, normed, preferred_element_type=jnp.float32).astype(
        jnp.bfloat16
    )
    outgoing = outgoing.reshape(experts, capacity, width)
    slice_width = width // lax.axis_size("tp")
    outgoing_part = lax.dynamic_slice_in_dim(
        outgoing, lax.axis_index("tp") * slice_width, slice_width, 2
    )
    arrived = lax.all_to_all(outgoing_part, "ep", split_axis=0, concat_axis=0, tiled=True)
    arrived = lax.all_gather(arrived, "tp", axis=2, tiled=True)
    arrived_rows = arrived.reshape(experts * capacity, width)
    gate_act = jnp.dot(arrived_rows, gate_weight[0], preferred_element_type=jnp.float32)
    up_act = jnp.dot(arrived_rows, up_weight[0], preferred_element_type=jnp.float32)
    hidden = (jax.nn.silu(gate_act) * up_act).astype(jnp.bfloat16)
    partial_value = jnp.dot(hidden, down_weight[0], preferred_element_type=jnp.float32)
    summed = lax.psum_scatter(
        partial_value.astype(jnp.bfloat16), "tp", scatter_dimension=1, tiled=True
    )
    returned = lax.all_to_all(
        summed.reshape(experts, capacity, summed.shape[1]),
        "ep",
        split_axis=0,
        concat_axis=0,
        tiled=True,
    )
    results = returned.reshape(experts * capacity, summed.shape[1]).astype(jnp.float32)
    mixing = jnp.sum(mix_weights[:, :, None] * by_choice.astype(jnp.float32), axis=1)
    mixed = jnp.dot(mixing, results, precision=lax.Precision.HIGHEST)
    squares = jnp.sum(mixed * mixed, axis=1)
    total = lax.psum(squares, "tp")
    scale = lax.rsqrt(total / width + epsilon)
    return (mixed * scale[:, None] * post_gain).astype(jnp.bfloat16)


def solution(mesh):
    in_specs = (
        P("ep", None),
        P("ep", None),
        P("ep", None),
        P(),
        P("ep", None, "tp"),
        P("ep", None, "tp"),
        P("ep", "tp", None),
        P("tp"),
    )
    out_specs = P("ep", "tp")
    S, NT = mesh.shape["ep"], mesh.shape["tp"]
    X = 2
    on_device = routed
    if (S, NT) == (4 * X, 2 * CORES):
        on_device = functools.partial(fused, S, X, NT)
    return jax.shard_map(
        on_device, mesh=mesh, in_specs=in_specs, out_specs=out_specs, check_vma=False
    )
```

time: 47.9 us -> 43.9 us (0.916)
  Pallas kernels: 46.3 us -> 42.2 us
    pallas_call x1, Pallas kernels: 46.3 us -> 42.2 us  [fused(): pl.pallas_call(functools.partial(fused_kernel, S, X, NT), out_shape=jax.S...]
where the time goes in v1:
time: 43.9 us; the launch traced here: 43.7 us
  Pallas kernels  42.2 us (96%)
  local copies, waits for them, and re-layouts  1.47 us (3%)
    pallas_call x1, Pallas kernels, fused(): pl.pallas_call(functools.partial(fused_kernel, S, X, NT), out_shape=jax.S...  42.2 us
    unnamed x1, local copies, waits for them, and re-layouts  1.47 us

profile of v1, /device:TPU:0, one launch (start us, length us, event | category | flops | bytes accessed | tf_op | source)
XLA Modules:
  0.0 43.7 jit_solution(9974002699517884386)
XLA Ops:
  0.0 42.2 %shard_map.82 = bf16[32,1024]{1,0:T(8,128)(2,1)} custom-call(bf16[32,4096]{1,0:T(8,128)(2,1)} %tokens_hbm.1, s32[4,32]{1,0:T(4,128)} %bitcast.6, f32[4,32]{1,0:T(4,128)} %bitcast.7, f32[1,4096]{1,0:T(1,128)} %bitcast.4, bf16[1,4096,512]{2,1,0:T(8,128)(2,1)} %gate_hbm.1, bf16[1,4096,512]{2,1,0:T(8,128)(2,1)} %up_hbm.1, bf16[1,512,4096]{2,1,0:T(8,128)(2,1)} %down_hbm.1, ...), custom_call_target="tpu_custom_call" | custom-call | tf_op jit(solution)/shard_map/pallas_call | solution.py:279
  42.2 1.5 %copy.10 = bf16[32,1024]{1,0:T(8,128)(2,1)} copy(bf16[32,1024]{1,0:T(8,128)(2,1)} %shard_map.82) | data formatting | bytes 131072
